TPU v7x, 512 devices: a whole 4x4x16 slice. The times are simulated.
512 devices in a mesh: dp: 4 (over x), kv: 64 (over z, y), tp: 2 (over core).
Axes of the slice: x: 4, y: 4, z: 16, core: 2. Of those that a mesh axis runs over, the one named last changes fastest.
Arguments:
- stream: bfloat16 [512, 2048], P('dp', ('kv', 'tp')), parts along dimension 0, may hold values from -40 to 40
- old_state: float32 [512, 8, 64, 128], P(('dp', 'kv'), 'tp'), parts along dimension 0, may hold values from -6 to 6
- decay_amounts: float32 [512, 512], P(('dp', 'kv'), 'tp'), parts along dimension 0, may hold values from 0.003 to 1
- first_gain: float32 [2048], replicated, may hold values from 0.1 to 1.9
- first_gate: bfloat16 [2048, 5632], P(None, ('kv', 'tp')), may hold values from -0.125 to 0.125
- first_up: bfloat16 [2048, 5632], P(None, ('kv', 'tp')), may hold values from -0.125 to 0.125
- first_down: bfloat16 [5632, 2048], P(('kv', 'tp')), may hold values from -0.078125 to 0.078125
- mixer_gain: float32 [2048], P('kv'), may hold values from 0.1 to 1.9
- query_weight: bfloat16 [2048, 512], P('kv', 'tp'), may hold values from -0.125 to 0.125
- key_weight: bfloat16 [2048, 512], P('kv', 'tp'), may hold values from -0.125 to 0.125
- decay_weight: bfloat16 [2048, 512], P('kv', 'tp'), may hold values from -0.5 to 0.5
- value_weight: bfloat16 [2048, 1024], P('kv', 'tp'), may hold values from -0.125 to 0.125
- output_gate_weight: bfloat16 [2048, 1024], P('kv', 'tp'), may hold values from -0.125 to 0.125
- head_gain: float32 [1024], P('tp'), may hold values from 0.1 to 1.9
- output_weight: bfloat16 [1024, 2048], P('tp', 'kv'), may hold values from -0.1875 to 0.1875
- second_gain: float32 [2048], replicated, may hold values from 0.1 to 1.9
- second_gate: bfloat16 [2048, 5632], P(None, ('kv', 'tp')), may hold values from -0.125 to 0.125
- second_up: bfloat16 [2048, 5632], P(None, ('kv', 'tp')), may hold values from -0.125 to 0.125
- second_down: bfloat16 [5632, 2048], P(('kv', 'tp')), may hold values from -0.078125 to 0.078125
Outputs:
- mixed_stream: bfloat16 [512, 2048], P('dp', ('kv', 'tp')), parts along dimension 0
- new_state: float32 [512, 8, 64, 128], P(('dp', 'kv'), 'tp'), parts along dimension 0
There are 4 independent parts, one for each index of `dp`. A program takes and returns all parts, laid end to end along the dimension named above; an argument that names none is the same for every part. Nothing has to cross between parts.
All inputs are finite; a program needn't handle non-finite values.
Results may differ from a plain program's by a relative error of at most 0.007.
Values may be sent and summed in bfloat16 or wider, within the bound.
A program may use at most 64 MiB of HBM per device.

v0:
```python
import math
import jax
import jax.numpy as jnp
from jax import lax
from jax.sharding import PartitionSpec as P

D = 2048
EPSILON = 1e-06
GATE_SOFTNESS = 16.0


def cut_along(value, dim, length):
    dims = value.shape
    parts = value.reshape(*dims[:dim], length, dims[dim] // length, *dims[dim + 1 :])
    return jnp.moveaxis(parts, dim, 0)


def summed_on_arrival(value, axis, dim):
    length = lax.axis_size(axis)
    parts = lax.all_to_all(cut_along(value, dim, length), axis, 0, 0, tiled=True)
    return jnp.sum(parts.astype(jnp.float32), axis=0)


def summed_on_arrival_2(value, axis, dim):
    parts = cut_along(value, dim, lax.axis_size(axis))
    arrived = lax.all_to_all(parts, axis, split_axis=0, concat_axis=0, tiled=True)
    return arrived.sum(axis=0)


def copy_for_each(value, axis):
    length = lax.axis_size(axis)
    return lax.all_to_all(
        jnp.broadcast_to(value[None], (length, *value.shape)), axis, 0, 0, tiled=True
    )


def in_order(parts, dim):
    dims = list(parts.shape[1:])
    dims[dim] *= parts.shape[0]
    return jnp.moveaxis(parts, 0, dim).reshape(dims)


def gathered_copies(value, axis, dim):
    parts = copy_for_each(value, axis)
    return in_order(parts, dim)


def in_one_piece(arrays, axis, dim, along):
    widths = [math.prod(a.shape[along:]) for a in arrays]
    both = jnp.concatenate(
        [a.reshape(*a.shape[:along], w) for a, w in zip(arrays, widths)], axis=along
    )
    result = summed_on_arrival_2(both, axis, dim)
    parts = jnp.split(result, [sum(widths[:k]) for k in range(1, len(widths))], axis=along)
    return tuple(
        (b.reshape(*result.shape[:along], *a.shape[along:]) for a, b in zip(arrays, parts))
    )


def half_block(stream, norm_gain, w_gate, w_up, w_down):
    wide = lax.all_gather(stream, ("kv", "tp"), axis=1, tiled=True).astype(jnp.float32)
    scaled = (wide * norm_gain).astype(jnp.bfloat16)
    gate_acc = jnp.dot(scaled, w_gate, preferred_element_type=jnp.float32)
    up_acc = jnp.dot(scaled, w_up, preferred_element_type=jnp.float32)
    square_acc = jnp.sum(wide * wide, axis=1)
    row_scale = lax.rsqrt(square_acc / norm_gain.shape[0] + EPSILON)[:, None]
    hidden = (jax.nn.silu(gate_acc * row_scale) * (up_acc * row_scale)).astype(jnp.bfloat16)
    partial_out = jnp.dot(hidden, w_down, preferred_element_type=jnp.float32)
    paired = summed_on_arrival(partial_out.astype(jnp.bfloat16), "tp", 0)
    blocked = summed_on_arrival_2(paired, "kv", 1)
    summed = lax.all_to_all(blocked, "tp", split_axis=1, concat_axis=0, tiled=True)
    return (stream.astype(jnp.float32) + 0.5 * summed).astype(jnp.bfloat16)


def body(
    stream,
    old_state,
    decay_amounts,
    first_gain,
    first_gate,
    first_up,
    first_down,
    mixer_gain,
    query_weight,
    key_weight,
    decay_weight,
    value_weight,
    output_gate_weight,
    head_gain,
    output_weight,
    second_gain,
    second_gate,
    second_up,
    second_down,
):
    middle = half_block(stream, first_gain, first_gate, first_up, first_down)
    paired_cols = gathered_copies(middle, "tp", 1)
    wide_cols = paired_cols.astype(jnp.float32)
    scaled = (wide_cols * mixer_gain).astype(jnp.bfloat16)
    query_part = jnp.dot(scaled, query_weight, preferred_element_type=jnp.float32)
    key_part = jnp.dot(scaled, key_weight, preferred_element_type=jnp.float32)
    decay_part = jnp.dot(scaled, decay_weight, preferred_element_type=jnp.float32)
    value_part = jnp.dot(scaled, value_weight, preferred_element_type=jnp.float32)
    outgate_part = jnp.dot(scaled, output_gate_weight, preferred_element_type=jnp.float32)
    local_rows = old_state.shape[0]
    local_heads = old_state.shape[1]
    key_dim = old_state.shape[2]
    value_dim = old_state.shape[3]
    query_sum, key_sum, decay_sum, value_sum, outgate_sum, own_squares = in_one_piece(
        (
            query_part,
            key_part,
            decay_part,
            value_part,
            outgate_part,
            jnp.sum(wide_cols * wide_cols, axis=1),
        ),
        "kv",
        0,
        1,
    )
    row_scale = lax.rsqrt(own_squares / D + EPSILON)[:, None]
    query = (query_sum * row_scale * key_dim ** (-0.5)).reshape(local_rows, local_heads, key_dim)
    keys = (key_sum * row_scale).reshape(local_rows, local_heads, key_dim)
    gate_logits = (decay_sum * row_scale).reshape(local_rows, local_heads, key_dim)
    values = (value_sum * row_scale).reshape(local_rows, local_heads, value_dim)
    decay_logarithm = jax.nn.log_sigmoid(gate_logits) / GATE_SOFTNESS - decay_amounts.reshape(
        local_rows, local_heads, key_dim
    )
    new_state = (
        jnp.exp(decay_logarithm)[..., None] * old_state + keys[..., None] * values[:, :, None, :]
    )
    readout = jnp.einsum("bhk,bhkv->bhv", query, new_state, precision=lax.Precision.HIGHEST)
    normed = readout * lax.rsqrt(jnp.mean(readout * readout, axis=-1, keepdims=True) + EPSILON)
    mixed_heads = (
        normed.reshape(local_rows, local_heads * value_dim)
        * head_gain
        * jax.nn.silu(outgate_sum * row_scale)
    ).astype(jnp.bfloat16)
    projected = jnp.dot(
        gathered_copies(mixed_heads, "kv", 0), output_weight, preferred_element_type=jnp.float32
    ).astype(jnp.bfloat16)
    attention_out = summed_on_arrival(
        lax.optimization_barrier(projected).astype(jnp.float32).astype(jnp.bfloat16), "tp", 1
    )
    after = (middle.astype(jnp.float32) + attention_out).astype(jnp.bfloat16)
    mixed_stream = half_block(after, second_gain, second_gate, second_up, second_down)
    return (mixed_stream, new_state)


def solution(mesh):
    in_specs = (
        P("dp", ("kv", "tp")),
        P(("dp", "kv"), "tp", None, None),
        P(("dp", "kv"), "tp"),
        P(),
        P(None, ("kv", "tp")),
        P(None, ("kv", "tp")),
        P(("kv", "tp"), None),
        P("kv"),
        P("kv", "tp"),
        P("kv", "tp"),
        P("kv", "tp"),
        P("kv", "tp"),
        P("kv", "tp"),
        P("tp"),
        P("tp", "kv"),
        P(),
        P(None, ("kv", "tp")),
        P(None, ("kv", "tp")),
        P(("kv", "tp"), None),
    )
    out_specs = (P("dp", ("kv", "tp")), P(("dp", "kv"), "tp", None, None))
    return jax.shard_map(body, mesh=mesh, in_specs=in_specs, out_specs=out_specs, check_vma=False)
```

profile of v0, /device:TPU:1, one launch (start us, length us, event | category | flops | bytes accessed | tf_op | source)
XLA Modules:
  0.0 385.9 jit_solution(13808392015291764144)
XLA Ops:
  0.6 91.5 %all_gather.6 = bf16[128,2048]{0,1:T(8,128)(2,1)S(1)} all-gather(bf16[128,16]{0,1:T(8,128)(2,1)} %param.19), channel_id=1, replica_groups=mesh['dp'=4,'kv'=64,'tp'=2] {'kv','tp'}, dimensions={1}, use_global_device_ids=true | all-gather | bytes 528384 | tf_op jit(solution)/shard_map/all_gather | solution.py:61
  92.2 0.3 fusion.5
  92.5 0.4 copy-done.13
  93.1 0.5 convolution_multiply_fusion.3
  93.6 0.4 copy-done.3
  94.0 0.8 convolution_convert_fusion.1
  94.8 3.9 %all_to_all.66 = bf16[2,64,2048]{2,1,0:T(8,128)(2,1)S(1)} all-to-all(bf16[2,64,2048]{2,1,0:T(8,128)(2,1)S(1)} %bitcast.78), channel_id=1, replica_groups=mesh['dp'=4,'kv'=64,'tp'=2] {'tp'}, dimensions={0} | all-to-all | bytes 1048576 | tf_op jit(solution)/shard_map/all_to_all | solution.py:20
  98.8 0.3 copy.89
  99.2 0.7 reshape.152
  99.9 40.3 %all_to_all.67 = f32[64,1,2048]{2,1,0:T(1,128)S(1)} all-to-all(f32[64,1,2048]{2,1,0:T(1,128)S(1)} %reshape.152), channel_id=1, replica_groups=mesh['dp'=4,'kv'=64,'tp'=2] {'kv'}, dimensions={0} | all-to-all | bytes 1048576 | tf_op jit(solution)/shard_map/all_to_all | solution.py:26
  140.1 0.5 broadcast.123
  140.6 1.9 reduce.4
  142.5 0.4 reshape.153
  143.1 6.1 %all_to_all.68 = f32[2,1,1024]{2,1,0:T(1,128)S(1)} all-to-all(f32[2,1,1024]{2,1,0:T(1,128)S(1)} %reshape.154), channel_id=1, replica_groups=mesh['dp'=4,'kv'=64,'tp'=2] {'tp'}, dimensions={0} | all-to-all | bytes 16384 | tf_op jit(solution)/shard_map/all_to_all | solution.py:71
  149.3 0.7 reduce.5
  150.1 0.6 copy-done.9
  150.7 3.7 all_to_all.69
  155.0 0.5 copy.93
  155.7 0.6 copy-done.10
  156.5 0.5 copy-done.11
  157.2 0.5 copy-done.12
  158.0 0.6 copy-done.6
  158.7 0.6 copy-done.7
  159.5 1.7 copy.94
  161.2 5.7 %all-to-all-start.4 = ((f32[64,2,1793]{2,1,0:T(2,128)}), f32[64,2,1793]{2,1,0:T(2,128)S(1)}, u32[]{:S(2)}, u32[]{:S(2)}) async-start(f32[64,2,1793]{2,1,0:T(2,128)} %copy.94), calls=%async_computation.4 | async-start | bytes 1966080 | tf_op jit(solution)/shard_map/all_to_all | solution.py:26
  167.0 49.8 %all-to-all-done.4 = f32[64,2,1793]{2,1,0:T(2,128)S(1)} async-done(((f32[64,2,1793]{2,1,0:T(2,128)}), f32[64,2,1793]{2,1,0:T(2,128)S(1)}, u32[]{:S(2)}, u32[]{:S(2)}) %all-to-all-start.4) | async-done | bytes 918048 | tf_op jit(solution)/shard_map/all_to_all | solution.py:26
  216.9 0.4 reduce_sum.94
  218.0 0.3 fusion.47
  218.5 0.6 copy-done.16
  219.3 23.2 %all_to_all.70 = bf16[64,2,512]{2,1,0:T(2,128)(2,1)S(1)} all-to-all(bf16[64,2,512]{2,1,0:T(2,128)(2,1)S(1)} %broadcast_in_dim.5), channel_id=1, replica_groups=mesh['dp'=4,'kv'=64,'tp'=2] {'kv'}, dimensions={0} | all-to-all | bytes 262144 | tf_op jit(solution)/shard_map/all_to_all | solution.py:32
  242.6 0.7 copy-done.8
  243.4 6.6 %all_to_all.71 = bf16[2,128,16]{1,2,0:T(8,128)(2,1)S(1)} all-to-all(bf16[2,128,16]{1,2,0:T(8,128)(2,1)S(1)} %bitcast.84), channel_id=1, replica_groups=mesh['dp'=4,'kv'=64,'tp'=2] {'tp'}, dimensions={0} | all-to-all | bytes 16384 | tf_op jit(solution)/shard_map/all_to_all | solution.py:20
  250.0 80.9 %all_gather.7 = bf16[128,2048]{0,1:T(8,128)(2,1)S(1)} all-gather(bf16[128,16]{0,1:T(8,128)(2,1)S(1)} %add_convert_fusion.1), channel_id=1, replica_groups=mesh['dp'=4,'kv'=64,'tp'=2] {'kv','tp'}, dimensions={1}, use_global_device_ids=true | all-gather | bytes 528384 | tf_op jit(solution)/shard_map/all_gather | solution.py:61
  330.9 0.3 fusion.7
  331.2 0.4 copy-done.14
  331.6 0.2 copy-done.19
  331.9 0.5 convolution_multiply_fusion.1
  332.4 0.5 copy-done.4
  332.9 0.8 convolution_convert_fusion
  333.7 3.9 %all_to_all.72 = bf16[2,64,2048]{2,1,0:T(8,128)(2,1)S(1)} all-to-all(bf16[2,64,2048]{2,1,0:T(8,128)(2,1)S(1)} %bitcast.79), channel_id=1, replica_groups=mesh['dp'=4,'kv'=64,'tp'=2] {'tp'}, dimensions={0} | all-to-all | bytes 1048576 | tf_op jit(solution)/shard_map/all_to_all | solution.py:20
  337.7 0.3 copy.96
  338.1 0.7 reshape.156
  338.7 37.1 %all_to_all.73 = f32[64,1,2048]{2,1,0:T(1,128)S(1)} all-to-all(f32[64,1,2048]{2,1,0:T(1,128)S(1)} %reshape.156), channel_id=1, replica_groups=mesh['dp'=4,'kv'=64,'tp'=2] {'kv'}, dimensions={0} | all-to-all | bytes 1048576 | tf_op jit(solution)/shard_map/all_to_all | solution.py:26
  375.8 1.9 reduce.6
  377.7 0.4 reshape.157
  378.3 6.1 %all_to_all.74 = f32[2,1,1024]{2,1,0:T(1,128)S(1)} all-to-all(f32[2,1,1024]{2,1,0:T(1,128)S(1)} %reshape.158), channel_id=1, replica_groups=mesh['dp'=4,'kv'=64,'tp'=2] {'tp'}, dimensions={0} | all-to-all | bytes 16384 | tf_op jit(solution)/shard_map/all_to_all | solution.py:71
  384.4 0.7 reduce.7
  385.3 0.6 add_convert_fusion
  (77 shorter events, 4.3 us)
Async XLA Ops:
  0.6 92.9 %copy-start = (bf16[44,2048]{1,0:T(8,128)(2,1)S(1)}, bf16[44,2048]{1,0:T(8,128)(2,1)}, u32[]{:S(2)}) copy-start(bf16[44,2048]{1,0:T(8,128)(2,1)} %param.25) | copy-start | bytes 540676
  92.2 0.7 copy-start.13
  92.2 0.9 copy-start.18
  93.1 0.9 copy-start.3
  150.0 0.7 copy-start.9
  155.0 0.7 copy-start.17
  155.6 0.7 copy-start.10
  156.3 0.7 copy-start.11
  157.1 0.7 copy-start.12
  157.8 0.8 copy-start.6
  158.5 0.8 copy-start.7
  161.2 5.7 %copy-start.15 = (f32[2,256]{1,0:T(2,128)S(1)}, f32[2,256]{1,0:T(2,128)}, u32[]{:S(2)}) copy-start(f32[2,256]{1,0:T(2,128)} %param.21) | copy-start | bytes 6148
  161.2 55.6 %all-to-all-start.4 = ((f32[64,2,1793]{2,1,0:T(2,128)}), f32[64,2,1793]{2,1,0:T(2,128)S(1)}, u32[]{:S(2)}, u32[]{:S(2)}) async-start(f32[64,2,1793]{2,1,0:T(2,128)} %copy.94), calls=%async_computation.4 | async-start | bytes 1966080 | tf_op jit(solution)/shard_map/all_to_all | solution.py:26
  167.0 50.8 %copy-start.2 = (f32[2,4,64,128]{3,2,1,0:T(8,128)S(1)}, f32[2,4,64,128]{3,2,1,0:T(8,128)}, u32[]{:S(2)}) copy-start(f32[2,4,64,128]{3,2,1,0:T(8,128)} %param.20) | copy-start | bytes 786436
  218.0 24.5 %copy-start.1 = (f32[2,4,64,128]{3,2,1,0:T(8,128)}, f32[2,4,64,128]{3,2,1,0:T(8,128)S(1)}, u32[]{:S(2)}) copy-start(f32[2,4,64,128]{3,2,1,0:T(8,128)S(1)} %multiply_add_fusion) | copy-start | bytes 786436
  218.4 0.7 copy-start.16
  242.5 0.8 copy-start.8
  330.9 0.7 copy-start.14
  330.9 0.9 copy-start.19
  331.9 0.9 copy-start.4
  331.9 1.0 copy-start.5
where the time goes:
time: 387 us; the launch traced here: 386 us
  blocking collectives  303 us (78%)
  waiting for transfers between devices  49.8 us (13%)
  local copies, waits for them, and re-layouts  14.2 us (4%)
  other arithmetic  7.92 us (2%)
  starting transfers between devices  5.69 us (1%)
    all_gather x2, blocking collectives, half_block(): lax.all_gather(stream, ('kv', 'tp'), axis=1, tiled=True).astype(jnp.float32)  172 us
    all_to_all x2, blocking collectives, summed_on_arrival_2(): lax.all_to_all(parts, axis, split_axis=0, concat_axis=0, tiled=True)  77.4 us
    all_to_all x1, waiting for transfers between devices, summed_on_arrival_2(): lax.all_to_all(parts, axis, split_axis=0, concat_axis=0, tiled=True)  49.8 us
    all_to_all x2, blocking collectives, copy_for_each(): lax.all_to_all(jnp.broadcast_to(value[None], (length, *value.shape)), axi...  26.9 us
    all_to_all x3, blocking collectives, summed_on_arrival(): lax.all_to_all(cut_along(value, dim, length), axis, 0, 0, tiled=True)  14.5 us
    all_to_all x2, blocking collectives, half_block(): lax.all_to_all(blocked, 'tp', split_axis=1, concat_axis=0, tiled=True)  12.3 us
    unnamed x48, local copies, waits for them, and re-layouts  9.68 us
  transfers between devices with their start and end apart: 1, of which 1 were waited for; matrix products, arithmetic and copies ran while one was open for 0% of the time, Pallas kernels for 0%

commit v1 on v0

--- a/solution.py
+++ b/solution.py
@@ -58,7 +58,10 @@
 
 
 def half_block(stream, norm_gain, w_gate, w_up, w_down):
-    wide = lax.all_gather(stream, ("kv", "tp"), axis=1, tiled=True).astype(jnp.float32)
+    wide = jnp.concatenate(
+        lax.all_to_all(jnp.stack([stream] * lax.axis_size(("kv", "tp"))), ("kv", "tp"), 0, 0),
+        axis=1,
+    ).astype(jnp.float32)
     scaled = (wide * norm_gain).astype(jnp.bfloat16)
     gate_acc = jnp.dot(scaled, w_gate, preferred_element_type=jnp.float32)
     up_acc = jnp.dot(scaled, w_up, preferred_element_type=jnp.float32)

time: 387 us -> 304 us (0.79)
  blocking collectives: 303 us -> 219 us
    all_gather x2 -> x0, blocking collectives: 172 us -> none  [half_block(): lax.all_gather(stream, ('kv', 'tp'), axis=1, tiled=True).astype(jnp.float32)]
    all_to_all x0 -> x2, blocking collectives: none -> 87.3 us  [half_block(): lax.all_to_all(jnp.stack([stream] * lax.axis_size(('kv', 'tp'))), ('kv',...]
where the time goes in v1:
time: 304 us; the launch traced here: 303 us
  blocking collectives  219 us (72%)
  waiting for transfers between devices  49.8 us (16%)
  local copies, waits for them, and re-layouts  16.3 us (5%)
  other arithmetic  8.59 us (3%)
  starting transfers between devices  5.69 us (2%)
    all_to_all x2, blocking collectives, half_block(): lax.all_to_all(jnp.stack([stream] * lax.axis_size(('kv', 'tp'))), ('kv',...  87.3 us
    all_to_all x2, blocking collectives, summed_on_arrival_2(): lax.all_to_all(parts, axis, split_axis=0, concat_axis=0, tiled=True)  76.8 us
    all_to_all x1, waiting for transfers between devices, summed_on_arrival_2(): lax.all_to_all(parts, axis, split_axis=0, concat_axis=0, tiled=True)  49.8 us
    all_to_all x2, blocking collectives, copy_for_each(): lax.all_to_all(jnp.broadcast_to(value[None], (length, *value.shape)), axi...  26.7 us
    all_to_all x3, blocking collectives, summed_on_arrival(): lax.all_to_all(cut_along(value, dim, length), axis, 0, 0, tiled=True)  15.9 us
    all_to_all x2, blocking collectives, half_block(): lax.all_to_all(blocked, 'tp', split_axis=1, concat_axis=0, tiled=True)  12.3 us
    unnamed x48, local copies, waits for them, and re-layouts  10.9 us
  transfers between devices with their start and end apart: 1, of which 1 were waited for; matrix products, arithmetic and copies ran while one was open for 0% of the time, Pallas kernels for 0%

profile of v1, /device:TPU:1, one launch (start us, length us, event | category | flops | bytes accessed | tf_op | source)
XLA Modules:
  0.0 303.2 jit_solution(17707296578034100339)
XLA Ops:
  0.6 0.8 stack.4
  1.4 51.0 %all_to_all.76 = bf16[128,128,16]{1,2,0:T(8,128)(2,1)S(1)} all-to-all(bf16[128,128,16]{1,2,0:T(8,128)(2,1)S(1)} %stack.4), channel_id=1, replica_groups=mesh['dp'=4,'kv'=64,'tp'=2] {'kv','tp'}, dimensions={0} | all-to-all | bytes 1048576 | tf_op jit(solution)/shard_map/all_to_all | solution.py:62
  52.8 0.4 copy-done.15
  53.2 0.3 fusion.5
  53.5 0.6 copy-done.3
  54.3 0.7 copy-done.5
  55.0 0.5 convolution_convert_fusion.1
  55.6 4.9 %all_to_all.77 = bf16[2,64,2048]{2,1,0:T(8,128)(2,1)S(1)} all-to-all(bf16[2,64,2048]{2,1,0:T(8,128)(2,1)S(1)} %bitcast.94), channel_id=1, replica_groups=mesh['dp'=4,'kv'=64,'tp'=2] {'tp'}, dimensions={0} | all-to-all | bytes 1048576 | tf_op jit(solution)/shard_map/all_to_all | solution.py:20
  60.5 0.3 copy.91
  60.9 0.7 reshape.166
  61.5 38.3 %all_to_all.78 = f32[64,1,2048]{2,1,0:T(1,128)S(1)} all-to-all(f32[64,1,2048]{2,1,0:T(1,128)S(1)} %reshape.166), channel_id=1, replica_groups=mesh['dp'=4,'kv'=64,'tp'=2] {'kv'}, dimensions={0} | all-to-all | bytes 1048576 | tf_op jit(solution)/shard_map/all_to_all | solution.py:26
  99.9 0.5 broadcast.127
  100.4 1.9 reduce.8
  102.3 0.4 reshape.167
  102.9 6.1 %all_to_all.79 = f32[2,1,1024]{2,1,0:T(1,128)S(1)} all-to-all(f32[2,1,1024]{2,1,0:T(1,128)S(1)} %reshape.168), channel_id=1, replica_groups=mesh['dp'=4,'kv'=64,'tp'=2] {'tp'}, dimensions={0} | all-to-all | bytes 16384 | tf_op jit(solution)/shard_map/all_to_all | solution.py:74
  109.0 0.7 reduce.9
  109.9 0.6 copy-done.11
  110.5 3.7 %all_to_all.80 = bf16[2,128,16]{1,2,0:T(8,128)(2,1)S(1)} all-to-all(bf16[2,128,16]{1,2,0:T(8,128)(2,1)S(1)} %broadcast_in_dim.4), channel_id=1, replica_groups=mesh['dp'=4,'kv'=64,'tp'=2] {'tp'}, dimensions={0} | all-to-all | bytes 16384 | tf_op jit(solution)/shard_map/all_to_all | solution.py:32
  114.7 0.5 copy.95
  115.4 0.6 copy-done.12
  116.3 0.5 copy-done.13
  117.0 0.5 copy-done.14
  117.7 0.6 copy-done.8
  118.5 0.5 copy-done.9
  119.3 1.7 copy.96
  121.0 5.7 %all-to-all-start.5 = ((f32[64,2,1793]{2,1,0:T(2,128)}), f32[64,2,1793]{2,1,0:T(2,128)S(1)}, u32[]{:S(2)}, u32[]{:S(2)}) async-start(f32[64,2,1793]{2,1,0:T(2,128)} %copy.96), calls=%async_computation.5 | async-start | bytes 1966080 | tf_op jit(solution)/shard_map/all_to_all | solution.py:26
  126.8 49.8 %all-to-all-done.5 = f32[64,2,1793]{2,1,0:T(2,128)S(1)} async-done(((f32[64,2,1793]{2,1,0:T(2,128)}), f32[64,2,1793]{2,1,0:T(2,128)S(1)}, u32[]{:S(2)}, u32[]{:S(2)}) %all-to-all-start.5) | async-done | bytes 918048 | tf_op jit(solution)/shard_map/all_to_all | solution.py:26
  176.6 0.4 reduce_sum.94
  177.8 0.3 fusion.39
  178.3 0.6 copy-done.18
  179.0 23.0 %all_to_all.81 = bf16[64,2,512]{2,1,0:T(2,128)(2,1)S(1)} all-to-all(bf16[64,2,512]{2,1,0:T(2,128)(2,1)S(1)} %broadcast_in_dim.5), channel_id=1, replica_groups=mesh['dp'=4,'kv'=64,'tp'=2] {'kv'}, dimensions={0} | all-to-all | bytes 262144 | tf_op jit(solution)/shard_map/all_to_all | solution.py:32
  202.2 0.7 copy-done.10
  203.0 6.6 %all_to_all.82 = bf16[2,128,16]{1,2,0:T(8,128)(2,1)S(1)} all-to-all(bf16[2,128,16]{1,2,0:T(8,128)(2,1)S(1)} %bitcast.100), channel_id=1, replica_groups=mesh['dp'=4,'kv'=64,'tp'=2] {'tp'}, dimensions={0} | all-to-all | bytes 16384 | tf_op jit(solution)/shard_map/all_to_all | solution.py:20
  209.6 36.2 %all_to_all.83 = bf16[128,128,16]{1,2,0:T(8,128)(2,1)S(1)} all-to-all(bf16[128,128,16]{1,2,0:T(8,128)(2,1)S(1)} %stack.5), channel_id=1, replica_groups=mesh['dp'=4,'kv'=64,'tp'=2] {'kv','tp'}, dimensions={0} | all-to-all | bytes 1048576 | tf_op jit(solution)/shard_map/all_to_all | solution.py:62
  246.2 0.4 copy-done.16
  246.6 0.3 fusion.4
  246.9 0.6 copy-done.4
  247.7 0.7 copy-done.6
  248.5 0.5 convolution_convert_fusion
  249.1 4.5 %all_to_all.84 = bf16[2,64,2048]{2,1,0:T(8,128)(2,1)S(1)} all-to-all(bf16[2,64,2048]{2,1,0:T(8,128)(2,1)S(1)} %bitcast.95), channel_id=1, replica_groups=mesh['dp'=4,'kv'=64,'tp'=2] {'tp'}, dimensions={0} | all-to-all | bytes 1048576 | tf_op jit(solution)/shard_map/all_to_all | solution.py:20
  253.6 0.3 copy.98
  254.0 0.7 reshape.170
  254.6 38.4 %all_to_all.85 = f32[64,1,2048]{2,1,0:T(1,128)S(1)} all-to-all(f32[64,1,2048]{2,1,0:T(1,128)S(1)} %reshape.170), channel_id=1, replica_groups=mesh['dp'=4,'kv'=64,'tp'=2] {'kv'}, dimensions={0} | all-to-all | bytes 1048576 | tf_op jit(solution)/shard_map/all_to_all | solution.py:26
  293.1 1.9 reduce.10
  295.0 0.4 reshape.171
  295.6 6.1 %all_to_all.86 = f32[2,1,1024]{2,1,0:T(1,128)S(1)} all-to-all(f32[2,1,1024]{2,1,0:T(1,128)S(1)} %reshape.172), channel_id=1, replica_groups=mesh['dp'=4,'kv'=64,'tp'=2] {'tp'}, dimensions={0} | all-to-all | bytes 16384 | tf_op jit(solution)/shard_map/all_to_all | solution.py:74
  301.7 0.7 reduce.11
  302.6 0.6 add_convert_fusion
  (81 shorter events, 5.1 us)
Async XLA Ops:
  0.6 53.7 %copy-start = (bf16[44,2048]{1,0:T(8,128)(2,1)S(1)}, bf16[44,2048]{1,0:T(8,128)(2,1)}, u32[]{:S(2)}) copy-start(bf16[44,2048]{1,0:T(8,128)(2,1)} %param.25) | copy-start | bytes 540676
  52.5 0.7 copy-start.15
  53.2 0.9 copy-start.3
  54.1 0.9 copy-start.5
  109.8 0.7 copy-start.11
  114.7 0.7 copy-start.19
  115.4 0.7 copy-start.12
  116.1 0.7 copy-start.13
  116.8 0.7 copy-start.14
  117.5 0.8 copy-start.8
  118.3 0.8 copy-start.9
  121.0 5.7 %copy-start.17 = (f32[2,256]{1,0:T(2,128)S(1)}, f32[2,256]{1,0:T(2,128)}, u32[]{:S(2)}) copy-start(f32[2,256]{1,0:T(2,128)} %param.21) | copy-start | bytes 6148
  121.0 55.6 %all-to-all-start.5 = ((f32[64,2,1793]{2,1,0:T(2,128)}), f32[64,2,1793]{2,1,0:T(2,128)S(1)}, u32[]{:S(2)}, u32[]{:S(2)}) async-start(f32[64,2,1793]{2,1,0:T(2,128)} %copy.96), calls=%async_computation.5 | async-start | bytes 1966080 | tf_op jit(solution)/shard_map/all_to_all | solution.py:26
  126.8 50.8 %copy-start.2 = (f32[2,4,64,128]{3,2,1,0:T(8,128)S(1)}, f32[2,4,64,128]{3,2,1,0:T(8,128)}, u32[]{:S(2)}) copy-start(f32[2,4,64,128]{3,2,1,0:T(8,128)} %param.20) | copy-start | bytes 786436
  177.8 24.3 %copy-start.1 = (f32[2,4,64,128]{3,2,1,0:T(8,128)}, f32[2,4,64,128]{3,2,1,0:T(8,128)S(1)}, u32[]{:S(2)}) copy-start(f32[2,4,64,128]{3,2,1,0:T(8,128)S(1)} %multiply_add_fusion) | copy-start | bytes 786436
  178.2 0.7 copy-start.18
  202.1 0.8 copy-start.10
  245.9 0.7 copy-start.16
  246.6 0.9 copy-start.4
  247.5 0.9 copy-start.6
  247.5 1.0 copy-start.7
